TPU v7x, 32 devices: a whole 2x2x4 slice. The times are simulated.
32 devices in a mesh: ep: 16 (over z, y, x), tp: 2 (over core).
Axes of the slice: x: 2, y: 2, z: 4, core: 2. Of those that a mesh axis runs over, the one named last changes fastest.
Arguments:
- tokens: bfloat16 [16, 2048], P('ep'), may hold values from -6 to 6
- norm_gain: float32 [2048], replicated, may hold values from 0.1 to 1.9
- w_query: bfloat16 [2048, 512], P('ep', 'tp'), may hold values from -0.125 to 0.125
- w_key: bfloat16 [2048, 512], P('ep', 'tp'), may hold values from -0.125 to 0.125
- w_value: bfloat16 [2048, 1024], P('ep', 'tp'), may hold values from -0.125 to 0.125
- w_outgate: bfloat16 [2048, 1024], P('ep', 'tp'), may hold values from -0.125 to 0.125
- decay_in: bfloat16 [2048, 16], replicated, may hold values from -0.125 to 0.125
- decay_out: bfloat16 [16, 512], P(None, 'tp'), may hold values from -1.5 to 1.5
- decay_bias: float32 [512], P('tp'), may hold values from -40 to 4
- gla_state: float32 [16, 2, 256, 512], P('ep', 'tp'), may hold values from -6 to 6
- head_gain: float32 [512], replicated, may hold values from 0.1 to 1.9
- w_output: bfloat16 [1024, 2048], P(None, 'ep'), may hold values from -0.1875 to 0.1875
- moe_gain: float32 [2048], replicated, may hold values from 0.1 to 1.9
- expert_ids: int32 [16, 6], replicated, may hold values from 0 to 15, all different within a row; in each aligned block of 16 rows (0 to 15, 16 to 31, ...) at most 12 rows name the same one
- route_weight: float32 [16, 6], replicated, may hold values from 0.2 to 1
- expert_gate: bfloat16 [16, 2048, 512], P('ep', None, 'tp'), may hold values from -0.125 to 0.125
- expert_up: bfloat16 [16, 2048, 512], P('ep', None, 'tp'), may hold values from -0.125 to 0.125
- expert_down: bfloat16 [16, 512, 2048], P('ep', 'tp'), may hold values from -0.25 to 0.25
- shared_gate: bfloat16 [2048, 512], P(None, 'tp'), may hold values from -0.125 to 0.125
- shared_up: bfloat16 [2048, 512], P(None, 'tp'), may hold values from -0.125 to 0.125
- shared_down: bfloat16 [512, 2048], P('tp'), may hold values from -0.25 to 0.25
Outputs:
- result: bfloat16 [16, 2048], P(None, 'ep')
- new_state: float32 [16, 2, 256, 512], P('ep', 'tp')
Inputs may be any that keep to these rules, and one draw needn't show every extreme that they name: `expert_ids`: each row names 6 different experts. No expert is named by more than 12 rows in all, a bound that some block reaches.
All inputs are finite; a program needn't handle non-finite values.
Results may differ from a plain program's by a relative error of at most 0.018.
Values may be sent and summed in bfloat16 or wider, within the bound.
No kernel may reach another device: no remote copies, remote signals or barrier semaphores. Data moves between devices by JAX's collectives and lax.ppermute only.
A program may use at most 64 MiB of HBM per device.

v0:
```python
import jax
import jax.numpy as jnp
from jax import lax
from jax.sharding import PartitionSpec as P

DK = 256
DV = 512
EPSILON = 1e-06
DECAY_TEMPER = 16.0


def rms_scale(values):
    return lax.rsqrt(jnp.mean(values * values, axis=-1, keepdims=True) + EPSILON)


def slot_positions(expert_ids, expert_count):
    flat_ids = expert_ids.reshape(-1)
    onehot = (flat_ids[:, None] == jnp.arange(expert_count, dtype=jnp.int32)[None, :]).astype(
        jnp.int32
    )
    before = jnp.cumsum(onehot, axis=0) - onehot
    position = jnp.sum(before * onehot, axis=1)
    return (flat_ids, position)


def expert_block(rows, moe_gain, gate_weight, up_weight, down_weight):
    row_float = rows.astype(jnp.float32)
    normal_rows = (row_float * rms_scale(row_float) * moe_gain).astype(jnp.bfloat16)
    gate_values = jnp.einsum(
        "ecd,edf->ecf", normal_rows, gate_weight, preferred_element_type=jnp.float32
    )
    upward = jnp.einsum("ecd,edf->ecf", normal_rows, up_weight, preferred_element_type=jnp.float32)
    active = (jax.nn.silu(gate_values) * upward).astype(jnp.bfloat16)
    return jnp.einsum(
        "ecf,efd->ecd", active, down_weight, preferred_element_type=jnp.float32
    ).astype(jnp.bfloat16)


def per_device(
    tokens,
    norm_gain,
    w_query,
    w_key,
    w_value,
    w_outgate,
    decay_in,
    decay_out,
    decay_bias,
    gla_state,
    head_gain,
    w_output,
    moe_gain,
    expert_ids,
    route_weight,
    expert_gate,
    expert_up,
    expert_down,
    shared_gate,
    shared_up,
    shared_down,
):
    ep_size = lax.axis_size("ep")
    tp_size = lax.axis_size("tp")
    seq_dev = tokens.shape[0]
    top_count = expert_ids.shape[1]
    exp_dev = expert_gate.shape[0]
    experts = exp_dev * ep_size
    all_rows = seq_dev * ep_size
    capacity = 2 * seq_dev * top_count // exp_dev
    heads_local = w_query.shape[1] // DK
    tok_float = tokens.astype(jnp.float32)
    normed = (tok_float * rms_scale(tok_float) * norm_gain).astype(jnp.bfloat16)
    span_sizes = (w_query.shape[1], w_key.shape[1], w_value.shape[1], w_outgate.shape[1])
    raw_columns, normed_columns = (
        lax.all_to_all(tokens, "ep", split_axis=1, concat_axis=0, tiled=True),
        lax.all_to_all(normed, "ep", split_axis=1, concat_axis=0, tiled=True),
    )
    joined = lax.psum_scatter(
        jnp.concatenate(
            [
                jnp.dot(normed_columns, weight, preferred_element_type=jnp.float32)
                for weight in (w_query, w_key, w_value, w_outgate)
            ],
            axis=1,
        ),
        "ep",
        scatter_dimension=0,
        tiled=True,
    )
    column_edges = [
        0,
        span_sizes[0],
        span_sizes[0] + span_sizes[1],
        span_sizes[0] + span_sizes[1] + span_sizes[2],
        sum(span_sizes),
    ]
    projected = tuple(
        (joined[:, column_edges[number] : column_edges[number + 1]] for number in range(4))
    )
    query_rows, key_rows, value_rows, gate_rows = (
        part_sum.astype(jnp.bfloat16) for part_sum in projected
    )
    decay_low = jnp.dot(normed, decay_in, preferred_element_type=jnp.float32).astype(jnp.bfloat16)
    decay_pre = jnp.dot(decay_low, decay_out, preferred_element_type=jnp.float32) + decay_bias
    decay_rate = jnp.exp(jax.nn.log_sigmoid(decay_pre) / DECAY_TEMPER).reshape(
        seq_dev, heads_local, DK
    )
    query_heads = query_rows.astype(jnp.float32).reshape(seq_dev, heads_local, DK) * DK ** (-0.5)
    key_heads = key_rows.astype(jnp.float32).reshape(seq_dev, heads_local, DK)
    value_heads = value_rows.astype(jnp.float32).reshape(seq_dev, heads_local, DV)
    new_state = (
        decay_rate[..., None] * gla_state + key_heads[..., None] * value_heads[:, :, None, :]
    )
    read_out = jnp.einsum("shk,shkv->shv", query_heads, new_state, precision=lax.Precision.HIGHEST)
    gate_heads = gate_rows.astype(jnp.float32).reshape(seq_dev, heads_local, DV)
    mixed_heads = (read_out * rms_scale(read_out) * head_gain * jax.nn.silu(gate_heads)).astype(
        jnp.bfloat16
    )
    head_weights = w_output.reshape(tp_size, heads_local * DV, w_output.shape[1])
    shard_rows = lax.all_gather(mixed_heads, ("ep", "tp"), axis=0, tiled=True)
    owners = lax.iota(jnp.int32, shard_rows.shape[0])
    select = (owners[:, None] % tp_size == lax.iota(jnp.int32, tp_size)[None, :]).astype(
        jnp.bfloat16
    )
    chosen = jnp.einsum(
        "mt,tcd->mcd", select, head_weights, preferred_element_type=jnp.float32
    ).astype(jnp.bfloat16)
    spread = jnp.einsum("msc,mcd->msd", shard_rows, chosen, preferred_element_type=jnp.float32)
    attention = (
        spread.reshape(ep_size, tp_size, seq_dev, -1)
        .sum(axis=1)
        .reshape(all_rows, -1)
        .astype(jnp.bfloat16)
    )
    hidden = (raw_columns.astype(jnp.float32) + attention.astype(jnp.float32)).astype(jnp.bfloat16)
    flat_ids, position = slot_positions(expert_ids, experts)
    owner_rows = lax.iota(jnp.int32, all_rows * top_count) // top_count
    slot_table = (
        jnp.full((experts, capacity), all_rows, jnp.int32).at[flat_ids, position].set(owner_rows)
    )
    padded = jnp.concatenate([hidden, jnp.zeros((1, hidden.shape[1]), jnp.bfloat16)], axis=0)
    routed_rows, shared_rows = (
        lax.all_to_all(padded[slot_table], "ep", split_axis=0, concat_axis=2, tiled=True),
        lax.all_to_all(
            hidden.reshape(ep_size, seq_dev, hidden.shape[1]),
            "ep",
            split_axis=0,
            concat_axis=2,
            tiled=True,
        ),
    )
    routed_part = expert_block(routed_rows, moe_gain, expert_gate, expert_up, expert_down)
    shared_part = expert_block(
        shared_rows, moe_gain, shared_gate[None], shared_up[None], shared_down[None]
    )
    routed_sum, shared_sum = (
        lax.psum(routed_part, "tp").astype(jnp.float32),
        lax.psum(shared_part, "tp").astype(jnp.float32),
    )
    routed_out = routed_sum.astype(jnp.bfloat16)
    shared_out = shared_sum.astype(jnp.bfloat16)
    back_routed, back_shared = (
        lax.all_to_all(routed_out, "ep", split_axis=2, concat_axis=0, tiled=True),
        lax.all_to_all(shared_out, "ep", split_axis=2, concat_axis=0, tiled=True),
    )
    picked = back_routed.reshape(experts * capacity, -1)[flat_ids * capacity + position]
    weighted = picked.astype(jnp.float32).reshape(all_rows, top_count, -1) * route_weight[..., None]
    moe_columns = jnp.sum(weighted, axis=1) + back_shared.reshape(all_rows, -1).astype(jnp.float32)
    result = (hidden.astype(jnp.float32) + moe_columns).astype(jnp.bfloat16)
    return (result, new_state)


def solution(mesh):
    return jax.shard_map(
        per_device,
        mesh=mesh,
        in_specs=(
            P("ep", None),
            P(),
            P("ep", "tp"),
            P("ep", "tp"),
            P("ep", "tp"),
            P("ep", "tp"),
            P(),
            P(None, "tp"),
            P("tp"),
            P("ep", "tp", None, None),
            P(),
            P(None, "ep"),
            P(),
            P(),
            P(),
            P("ep", None, "tp"),
            P("ep", None, "tp"),
            P("ep", "tp", None),
            P(None, "tp"),
            P(None, "tp"),
            P("tp", None),
        ),
        out_specs=(P(None, "ep"), P("ep", "tp", None, None)),
        check_vma=False,
    )
```

profile of v0, /device:TPU:0, one launch (start us, length us, event | category | flops | bytes accessed | tf_op | source)
XLA Modules:
  0.0 244.8 jit_solution(1949194534503189319)
XLA Ops:
  0.6 0.0 copy-start
  0.6 0.0 copy-start.11
  0.7 1.4 multiply_reduce_fusion.2
  2.8 1.3 convert_bitcast_fusion.3
  4.1 8.3 %all-to-all-start.1 = ((bf16[1,16,128]{2,0,1:T(2,128)(2,1)}), bf16[1,16,128]{2,0,1:T(2,128)(2,1)S(1)}, u32[]{:S(2)}, u32[]{:S(2)}) async-start(bf16[1,16,128]{2,0,1:T(2,128)(2,1)} %convert_bitcast_fusion.3), calls=%async_computation.1 | async-start | bytes 16384 | tf_op jit(solution)/shard_map/all_to_all | solution.py:76
  12.5 0.8 copy.66
  13.3 0.1 eq.33
  13.4 0.1 reshape.455
  13.5 0.1 fusion.20
  13.5 0.0 copy-start.10
  13.6 0.1 reduce_window_sum.11
  13.7 0.2 select_reduce_fusion
  13.9 5.4 %scatter_fusion = s32[16,12]{1,0:T(8,128)S(1)} fusion(s32[16,12]{1,0:T(8,128)S(1)} %broadcast_in_dim.7, s32[96]{0:T(128)S(1)} %get-tuple-element.7, s32[96]{0:T(128)S(1)} %and_select_fusion), kind=kCustom, calls=%fused_computation.2 | custom fusion | bytes 1920 | tf_op jit(solution)/shard_map/scatter | solution.py:139
  19.3 0.1 reshape.472
  19.4 1.1 fusion.11
  20.5 0.7 fusion.51
  21.2 4.2 %convolution_convert_fusion = bf16[32,512,128]{2,0,1:T(8,128)(2,1)} fusion(bf16[2,512,128]{2,1,0:T(8,128)(2,1)} %bitcast.143, s32[32]{0:T(128)S(1)} %and_select_fusion.1), kind=kOutput, calls=%fused_computation.5 | convolution fusion | flops 10485824 | bytes 4456576 | tf_op jit(solution)/shard_map/mt,tcd->mcd/dot_general | solution.py:125
  25.5 0.6 dynamic-slice
  26.0 0.0 all-to-all-done.1
  26.1 6.9 %all-to-all-start = ((bf16[1,16,128]{2,0,1:T(2,128)(2,1)}), bf16[1,16,128]{2,0,1:T(2,128)(2,1)S(1)}, u32[]{:S(2)}, u32[]{:S(2)}) async-start(bf16[1,16,128]{2,0,1:T(2,128)(2,1)} %bitcast), calls=%async_computation | async-start | bytes 16384 | tf_op jit(solution)/shard_map/all_to_all | solution.py:75
  33.0 0.1 fusion.36
  33.1 0.1 fusion.38
  33.3 0.1 fusion.40
  33.4 0.1 fusion.42
  33.5 78.2 %all-reduce.1 = bf16[16,1536]{1,0:T(8,128)(2,1)S(1)} all-reduce(f32[16,1536]{1,0:T(8,128)S(1)} %pad_maximum_fusion), channel_id=3, replica_groups=mesh['ep'=16,'tp'=2] {'ep'}, use_global_device_ids=true, to_apply=%region_1.0.clone | all-reduce | flops 24576 | bytes 147456
  111.7 0.7 dynamic-slice_convert_fusion
  112.4 1.2 multiply_add_fusion
  113.6 0.0 copy-start.1
  113.6 0.8 copy-done.1
  114.4 0.4 fusion.12
  114.8 0.6 multiply_reduce_fusion.3
  116.1 36.5 %all-gather.1 = bf16[32,1,512]{2,1,0:T(2,128)(2,1)S(1)} all-gather(bf16[1,1,512]{2,1,0:T(2,128)(2,1)S(1)} %reshape.496), channel_id=2, replica_groups=mesh['ep'=16,'tp'=2] {'ep','tp'}, dimensions={0}, use_global_device_ids=true | all-gather | bytes 33792 | tf_op jit(solution)/shard_map/all_gather | solution.py:120
  152.6 6.4 %fusion = f32[32,1,128]{2,1,0:T(1,128)S(1)} fusion(bf16[32,512,128]{2,0,1:T(8,128)(2,1)} %convolution_convert_fusion, bf16[32,1,512]{2,1,0:T(2,128)(2,1)S(1)} %all-gather.1), kind=kOutput, calls=%fused_computation.3 | convolution fusion | flops 4194304 | bytes 4243456 | tf_op jit(solution)/shard_map/msc,mcd->msd/dot_general | solution.py:128
  159.1 0.6 copy.73
  159.7 3.4 %all-to-all-start.4 = ((bf16[16,1,128]{2,1,0:T(2,128)(2,1)}), bf16[16,1,128]{2,1,0:T(2,128)(2,1)S(1)}, u32[]{:S(2)}, u32[]{:S(2)}) async-start(bf16[16,1,128]{2,1,0:T(2,128)(2,1)} %copy.73), calls=%async_computation.4 | async-start | bytes 16384 | tf_op jit(solution)/shard_map/all_to_all | solution.py:144
  163.2 0.8 gather_fusion
  163.9 0.6 reshape.471
  164.6 5.8 %all-to-all-done.4 = bf16[16,1,128]{2,1,0:T(2,128)(2,1)S(1)} async-done(((bf16[16,1,128]{2,1,0:T(2,128)(2,1)}), bf16[16,1,128]{2,1,0:T(2,128)(2,1)S(1)}, u32[]{:S(2)}, u32[]{:S(2)}) %all-to-all-start.4) | async-done | bytes 4128 | tf_op jit(solution)/shard_map/all_to_all | solution.py:144
  170.4 3.5 %all-to-all-start.2 = ((bf16[16,12,128]{2,1,0:T(8,128)(2,1)}), bf16[16,12,128]{2,1,0:T(8,128)(2,1)S(1)}, u32[]{:S(2)}, u32[]{:S(2)}) async-start(bf16[16,12,128]{2,1,0:T(8,128)(2,1)} %reshape.471), calls=%async_computation.2 | async-start | bytes 131072 | tf_op jit(solution)/shard_map/all_to_all | solution.py:143
  173.9 0.6 multiply_reduce_fusion.1
  175.3 0.2 fusion.64
  175.5 0.3 fusion.65
  175.8 1.5 fusion.66
  177.3 4.1 %all-to-all-done.2 = bf16[16,12,128]{2,1,0:T(8,128)(2,1)S(1)} async-done(((bf16[16,12,128]{2,1,0:T(8,128)(2,1)}), bf16[16,12,128]{2,1,0:T(8,128)(2,1)S(1)}, u32[]{:S(2)}, u32[]{:S(2)}) %all-to-all-start.2) | async-done | bytes 49184 | tf_op jit(solution)/shard_map/all_to_all | solution.py:143
  181.4 0.1 fusion.15
  181.5 0.1 fusion.18
  181.7 1.5 fusion.9
  183.2 2.0 fusion.2
  185.1 3.6 %all-reduce.2 = (bf16[1,12,2048]{2,1,0:T(8,128)(2,1)S(1)}, bf16[1,1,2048]{2,1,0:T(2,128)(2,1)S(1)}) all-reduce(bf16[1,12,2048]{2,1,0:T(8,128)(2,1)S(1)} %fusion.2, bf16[1,1,2048]{2,1,0:T(2,128)(2,1)S(1)} %convert_element_type.218), channel_id=1, replica_groups=mesh['ep'=16,'tp'=2] {'tp'}, use_global_device_ids=true, to_apply=%region_8.9 | all-reduce | flops 26624 | bytes 106496 | tf_op jit(solution)/shard_map/psum | solution.py:157
  188.7 2.1 copy.74
  190.8 3.8 %all-to-all-start.5 = ((bf16[1,1,2048]{1,0,2:T(2,128)(2,1)}), bf16[1,1,2048]{1,0,2:T(2,128)(2,1)S(1)}, u32[]{:S(2)}, u32[]{:S(2)}) async-start(bf16[1,1,2048]{1,0,2:T(2,128)(2,1)} %copy.74), calls=%async_computation.5 | async-start | bytes 2097152 | tf_op jit(solution)/shard_map/all_to_all | solution.py:164
  194.6 0.1 copy.72
  194.7 0.8 copy.69
  195.6 0.5 broadcast.257
  196.1 12.4 %reduce.11 = bf16[2048,12]{1,0:T(8,128)(2,1)} reduce(bf16[2048,1,12]{2,1,0:T(2,128)(2,1)S(1)} %bitcast.139, bf16[]{:T(256)} %broadcast.257), dimensions={1}, to_apply=%bitcast.122.reduce_sub_computation | reduce | bytes 98306
  208.4 2.4 reshape.519
  210.9 8.5 %all-to-all-done.5 = bf16[1,1,2048]{1,0,2:T(2,128)(2,1)S(1)} async-done(((bf16[1,1,2048]{1,0,2:T(2,128)(2,1)}), bf16[1,1,2048]{1,0,2:T(2,128)(2,1)S(1)}, u32[]{:S(2)}, u32[]{:S(2)}) %all-to-all-start.5) | async-done | bytes 4128 | tf_op jit(solution)/shard_map/all_to_all | solution.py:164
  219.3 6.8 %all-to-all-start.3 = ((bf16[16,2,768]{2,1,0:T(2,128)(2,1)}), bf16[16,2,768]{2,1,0:T(2,128)(2,1)S(1)}, u32[]{:S(2)}, u32[]{:S(2)}) async-start(bf16[16,2,768]{2,1,0:T(2,128)(2,1)} %reshape.519), calls=%async_computation.3 | async-start | bytes 98304 | tf_op jit(solution)/shard_map/all_to_all | solution.py:163
  226.1 15.2 %convert_reduce_fusion = f32[2048]{0:T(1024)S(1)} fusion(bf16[1,1,2048]{1,0,2:T(2,128)(2,1)S(1)} %all-to-all-done.5), kind=kLoop, calls=%fused_computation.17 | loop fusion | flops 2048 | bytes 12288 | tf_op jit(solution)/shard_map/convert_element_type | solution.py:168
  241.3 1.4 reshape.520
  242.8 0.6 copy.70
  243.4 0.7 gather_fusion.1
  244.1 0.1 multiply_reduce_fusion
  244.2 0.6 fusion.30
  (54 shorter events, 0.3 us)
Async XLA Ops:
  0.6 182.6 %copy-start = (bf16[1,256,2048]{2,1,0:T(8,128)(2,1)S(1)}, bf16[1,256,2048]{2,1,0:T(8,128)(2,1)}, u32[]{:S(2)}) copy-start(bf16[1,256,2048]{2,1,0:T(8,128)(2,1)} %param.38) | copy-start | bytes 3145732
  0.6 24.8 %copy-start.11 = (u32[32]{0:T(128)S(1)}, u32[32]{0:T(128)}, u32[]{:S(2)}) copy-start(u32[32]{0:T(128)} %constant.104) | copy-start | bytes 388
  0.7 32.3 %copy-start.4 = (bf16[128,512]{1,0:T(8,128)(2,1)S(1)}, bf16[128,512]{1,0:T(8,128)(2,1)}, u32[]{:S(2)}) copy-start(bf16[128,512]{1,0:T(8,128)(2,1)} %param.26) | copy-start | bytes 393220
  0.7 32.4 %copy-start.5 = (bf16[128,512]{1,0:T(8,128)(2,1)S(1)}, bf16[128,512]{1,0:T(8,128)(2,1)}, u32[]{:S(2)}) copy-start(bf16[128,512]{1,0:T(8,128)(2,1)} %param.25) | copy-start | bytes 393220
  0.7 32.6 %copy-start.6 = (bf16[128,256]{1,0:T(8,128)(2,1)S(1)}, bf16[128,256]{1,0:T(8,128)(2,1)}, u32[]{:S(2)}) copy-start(bf16[128,256]{1,0:T(8,128)(2,1)} %param.24) | copy-start | bytes 196612
  0.7 32.7 %copy-start.7 = (bf16[128,256]{1,0:T(8,128)(2,1)S(1)}, bf16[128,256]{1,0:T(8,128)(2,1)}, u32[]{:S(2)}) copy-start(bf16[128,256]{1,0:T(8,128)(2,1)} %param.23) | copy-start | bytes 196612
  4.1 21.9 %all-to-all-start.1 = ((bf16[1,16,128]{2,0,1:T(2,128)(2,1)}), bf16[1,16,128]{2,0,1:T(2,128)(2,1)S(1)}, u32[]{:S(2)}, u32[]{:S(2)}) async-start(bf16[1,16,128]{2,0,1:T(2,128)(2,1)} %convert_bitcast_fusion.3), calls=%async_computation.1 | async-start | bytes 16384 | tf_op jit(solution)/shard_map/all_to_all | solution.py:76
  13.5 102.5 %copy-start.10 = (f32[512]{0:T(512)S(1)}, f32[512]{0:T(512)}, u32[]{:S(2)}) copy-start(f32[512]{0:T(512)} %param.31) | copy-start | bytes 6148
  25.4 149.8 %copy-start.8 = (f32[2048]{0:T(1024)S(1)}, f32[2048]{0:T(1024)}, u32[]{:S(2)}) copy-start(f32[2048]{0:T(1024)} %param.33) | copy-start | bytes 24580
  25.4 149.8 %copy-start.2 = (bf16[2048,256]{1,0:T(8,128)(2,1)S(1)}, bf16[2048,256]{1,0:T(8,128)(2,1)}, u32[]{:S(2)}) copy-start(bf16[2048,256]{1,0:T(8,128)(2,1)} %param.39) | copy-start | bytes 3145732
  26.1 133.0 %all-to-all-start = ((bf16[1,16,128]{2,0,1:T(2,128)(2,1)}), bf16[1,16,128]{2,0,1:T(2,128)(2,1)S(1)}, u32[]{:S(2)}, u32[]{:S(2)}) async-start(bf16[1,16,128]{2,0,1:T(2,128)(2,1)} %bitcast), calls=%async_computation | async-start | bytes 16384 | tf_op jit(solution)/shard_map/all_to_all | solution.py:75
  33.5 142.0 %copy-start.3 = (bf16[2048,256]{1,0:T(8,128)(2,1)S(1)}, bf16[2048,256]{1,0:T(8,128)(2,1)}, u32[]{:S(2)}) copy-start(bf16[2048,256]{1,0:T(8,128)(2,1)} %param.40) | copy-start | bytes 3145732
  113.6 0.8 copy-start.1
  159.7 10.7 %all-to-all-start.4 = ((bf16[16,1,128]{2,1,0:T(2,128)(2,1)}), bf16[16,1,128]{2,1,0:T(2,128)(2,1)S(1)}, u32[]{:S(2)}, u32[]{:S(2)}) async-start(bf16[16,1,128]{2,1,0:T(2,128)(2,1)} %copy.73), calls=%async_computation.4 | async-start | bytes 16384 | tf_op jit(solution)/shard_map/all_to_all | solution.py:144
  170.4 11.0 %all-to-all-start.2 = ((bf16[16,12,128]{2,1,0:T(8,128)(2,1)}), bf16[16,12,128]{2,1,0:T(8,128)(2,1)S(1)}, u32[]{:S(2)}, u32[]{:S(2)}) async-start(bf16[16,12,128]{2,1,0:T(8,128)(2,1)} %reshape.471), calls=%async_computation.2 | async-start | bytes 131072 | tf_op jit(solution)/shard_map/all_to_all | solution.py:143
  175.8 18.9 %copy-start.9 = (f32[16,6]{0,1:T(8,128)S(1)}, f32[16,6]{0,1:T(8,128)}, u32[]{:S(2)}) copy-start(f32[16,6]{0,1:T(8,128)} %param.35) | copy-start | bytes 1156
  190.8 28.6 %all-to-all-start.5 = ((bf16[1,1,2048]{1,0,2:T(2,128)(2,1)}), bf16[1,1,2048]{1,0,2:T(2,128)(2,1)S(1)}, u32[]{:S(2)}, u32[]{:S(2)}) async-start(bf16[1,1,2048]{1,0,2:T(2,128)(2,1)} %copy.74), calls=%async_computation.5 | async-start | bytes 2097152 | tf_op jit(solution)/shard_map/all_to_all | solution.py:164
  219.3 22.0 %all-to-all-start.3 = ((bf16[16,2,768]{2,1,0:T(2,128)(2,1)}), bf16[16,2,768]{2,1,0:T(2,128)(2,1)S(1)}, u32[]{:S(2)}, u32[]{:S(2)}) async-start(bf16[16,2,768]{2,1,0:T(2,128)(2,1)} %reshape.519), calls=%async_computation.3 | async-start | bytes 98304 | tf_op jit(solution)/shard_map/all_to_all | solution.py:163
where the time goes:
time: 246 us; the launch traced here: 245 us
  blocking collectives  118 us (48%)
  other arithmetic  34.9 us (14%)
  starting transfers between devices  32.8 us (13%)
  local copies, waits for them, and re-layouts  19.3 us (8%)
  waiting for transfers between devices  18.4 us (7%)
  matrix products  18 us (7%)
  between operations  3.2 us (1%)
    unnamed x1, blocking collectives  78.2 us
    all_gather x1, blocking collectives, per_device(): shard_rows = lax.all_gather(mixed_heads, ('ep', 'tp'), axis=0, tiled=True)  36.5 us
    convert_element_type x1, other arithmetic, per_device(): back_shared.reshape(all_rows, -1).astype(jnp.float32)  15.2 us
    unnamed x1, other arithmetic  12.4 us
    all_to_all x1, waiting for transfers between devices, per_device(): lax.all_to_all(shared_out, 'ep', split_axis=2, concat_axis=0, tiled=True)  8.46 us
    all_to_all x1, starting transfers between devices, per_device(): lax.all_to_all(normed, 'ep', split_axis=1, concat_axis=0, tiled=True)  8.34 us
    all_to_all x1, starting transfers between devices, per_device(): lax.all_to_all(tokens, 'ep', split_axis=1, concat_axis=0, tiled=True)  6.91 us
    all_to_all x1, starting transfers between devices, per_device(): lax.all_to_all(routed_out, 'ep', split_axis=2, concat_axis=0, tiled=True)  6.75 us
  transfers between devices with their start and end apart: 6, of which 3 were waited for; matrix products, arithmetic and copies ran while one was open for 24% of the time, Pallas kernels for 0%

commit v1 on v0

--- a/solution.py
+++ b/solution.py
@@ -161,7 +161,12 @@
     shared_out = shared_sum.astype(jnp.bfloat16)
     back_routed, back_shared = (
         lax.all_to_all(routed_out, "ep", split_axis=2, concat_axis=0, tiled=True),
-        lax.all_to_all(shared_out, "ep", split_axis=2, concat_axis=0, tiled=True),
+        jnp.concatenate(
+            lax.all_to_all(
+                jnp.stack(jnp.split(shared_out, lax.axis_size("ep"), axis=2)), "ep", 0, 0
+            ),
+            axis=0,
+        ),
     )
     picked = back_routed.reshape(experts * capacity, -1)[flat_ids * capacity + position]
     weighted = picked.astype(jnp.float32).reshape(all_rows, top_count, -1) * route_weight[..., None]

time: 246 us -> 233 us (0.947)
  other arithmetic: 34.9 us -> 17.8 us
  local copies, waits for them, and re-layouts: 19.3 us -> 24.3 us
  starting transfers between devices: 32.8 us -> 29.7 us
    convert_element_type x1 -> x0, other arithmetic: 15.2 us -> none  [per_device(): back_shared.reshape(all_rows, -1).astype(jnp.float32)]
    all_to_all x1, waiting for transfers between devices: 0.01 us -> 6.89 us  [per_device(): lax.all_to_all(routed_out, 'ep', split_axis=2, concat_axis=0, tiled=True)]
    unnamed x35 -> x50, local copies, waits for them, and re-layouts: 6.68 us -> 13.2 us
    all_to_all x1, waiting for transfers between devices: 8.46 us -> 4.37 us  [per_device(): lax.all_to_all(jnp.stack(jnp.split(shared_out, lax.axis_size('ep'), axis=...]
    all_to_all x1, starting transfers between devices: 6.75 us -> 4.01 us  [per_device(): lax.all_to_all(routed_out, 'ep', split_axis=2, concat_axis=0, tiled=True)]
  transfers between devices with their start and end apart: 6 -> 6, of which waited for: 3 -> 4; matrix products, arithmetic and copies ran while one was open for 24% -> 13% of each run, Pallas kernels for 0% -> 0%
where the time goes in v1:
time: 233 us
  blocking collectives  118 us (51%)
  starting transfers between devices  29.7 us (13%)
  local copies, waits for them, and re-layouts  24.3 us (10%)
  waiting for transfers between devices  20 us (9%)
  matrix products  19.3 us (8%)
  other arithmetic  17.8 us (8%)
  between operations  3.23 us (1%)
    unnamed x1, blocking collectives  78 us
    all_gather x1, blocking collectives, per_device(): shard_rows = lax.all_gather(mixed_heads, ('ep', 'tp'), axis=0, tiled=True)  36.5 us
    unnamed x50, local copies, waits for them, and re-layouts  13.2 us
    unnamed x1, other arithmetic  11.5 us
    all_to_all x1, starting transfers between devices, per_device(): lax.all_to_all(normed, 'ep', split_axis=1, concat_axis=0, tiled=True)  8.34 us
    all_to_all x1, starting transfers between devices, per_device(): lax.all_to_all(tokens, 'ep', split_axis=1, concat_axis=0, tiled=True)  6.91 us
    all_to_all x1, waiting for transfers between devices, per_device(): lax.all_to_all(routed_out, 'ep', split_axis=2, concat_axis=0, tiled=True)  6.89 us
    dot_general x1, matrix products, per_device(): jnp.einsum('msc,mcd->msd', shard_rows, chosen, preferred_element_type=jnp...  6.42 us
  transfers between devices with their start and end apart: 6, of which 4 were waited for; matrix products, arithmetic and copies ran while one was open for 13% of the time, Pallas kernels for 0%

profile of v1, /device:TPU:0, one launch (start us, length us, event | category | flops | bytes accessed | tf_op | source)
XLA Modules:
  0.0 232.6 jit_solution(17095565702015999689)
XLA Ops:
  0.7 1.4 multiply_reduce_fusion.2
  2.9 1.3 convert_bitcast_fusion.3
  4.2 8.3 %all-to-all-start.1 = ((bf16[1,16,128]{2,0,1:T(2,128)(2,1)}), bf16[1,16,128]{2,0,1:T(2,128)(2,1)S(1)}, u32[]{:S(2)}, u32[]{:S(2)}) async-start(bf16[1,16,128]{2,0,1:T(2,128)(2,1)} %convert_bitcast_fusion.3), calls=%async_computation.1 | async-start | bytes 16384 | tf_op jit(solution)/shard_map/all_to_all | solution.py:76
  12.5 0.8 copy.99
  13.6 0.1 reduce_window_sum.11
  13.7 0.2 select_reduce_fusion
  13.9 5.4 %scatter_fusion = s32[16,12]{1,0:T(8,128)S(1)} fusion(s32[16,12]{1,0:T(8,128)S(1)} %broadcast_in_dim.7, s32[96]{0:T(128)S(1)} %get-tuple-element.7, s32[96]{0:T(128)S(1)} %and_select_fusion), kind=kCustom, calls=%fused_computation.2 | custom fusion | bytes 1920 | tf_op jit(solution)/shard_map/scatter | solution.py:139
  19.5 1.1 fusion.11
  20.6 0.7 fusion.51
  21.3 4.2 %convolution_convert_fusion = bf16[32,512,128]{2,0,1:T(8,128)(2,1)} fusion(bf16[2,512,128]{2,1,0:T(8,128)(2,1)} %bitcast.204, s32[32]{0:T(128)S(1)} %and_select_fusion.1), kind=kOutput, calls=%fused_computation.5 | convolution fusion | flops 10485824 | bytes 4456576 | tf_op jit(solution)/shard_map/mt,tcd->mcd/dot_general | solution.py:125
  25.6 0.6 dynamic-slice
  26.2 6.9 %all-to-all-start = ((bf16[1,16,128]{2,0,1:T(2,128)(2,1)}), bf16[1,16,128]{2,0,1:T(2,128)(2,1)S(1)}, u32[]{:S(2)}, u32[]{:S(2)}) async-start(bf16[1,16,128]{2,0,1:T(2,128)(2,1)} %bitcast), calls=%async_computation | async-start | bytes 16384 | tf_op jit(solution)/shard_map/all_to_all | solution.py:75
  33.4 0.1 fusion.40
  33.5 0.1 fusion.42
  33.7 78.0 %all-reduce.1 = bf16[16,1536]{1,0:T(8,128)(2,1)S(1)} all-reduce(f32[16,1536]{1,0:T(8,128)S(1)} %pad_maximum_fusion), channel_id=3, replica_groups=mesh['ep'=16,'tp'=2] {'ep'}, use_global_device_ids=true, to_apply=%region_1.0.clone | all-reduce | flops 24576 | bytes 147456
  111.7 0.7 dynamic-slice_convert_fusion
  112.4 0.1 multiply_add_fusion
  112.6 0.4 fusion.12
  113.0 0.6 multiply_reduce_fusion.3
  114.3 36.5 %all-gather.1 = bf16[32,1,512]{2,1,0:T(2,128)(2,1)S(1)} all-gather(bf16[1,1,512]{2,1,0:T(2,128)(2,1)S(1)} %reshape.491), channel_id=2, replica_groups=mesh['ep'=16,'tp'=2] {'ep','tp'}, dimensions={0}, use_global_device_ids=true | all-gather | bytes 33792 | tf_op jit(solution)/shard_map/all_gather | solution.py:120
  150.8 6.4 %fusion = f32[32,1,128]{2,1,0:T(1,128)S(1)} fusion(bf16[32,512,128]{2,0,1:T(8,128)(2,1)} %convolution_convert_fusion, bf16[32,1,512]{2,1,0:T(2,128)(2,1)S(1)} %all-gather.1), kind=kOutput, calls=%fused_computation.3 | convolution fusion | flops 4194304 | bytes 4243456 | tf_op jit(solution)/shard_map/msc,mcd->msd/dot_general | solution.py:128
  157.3 0.6 copy.106
  157.9 3.4 %all-to-all-start.4 = ((bf16[16,1,128]{2,1,0:T(2,128)(2,1)}), bf16[16,1,128]{2,1,0:T(2,128)(2,1)S(1)}, u32[]{:S(2)}, u32[]{:S(2)}) async-start(bf16[16,1,128]{2,1,0:T(2,128)(2,1)} %copy.106), calls=%async_computation.4 | async-start | bytes 16384 | tf_op jit(solution)/shard_map/all_to_all | solution.py:144
  161.4 0.8 gather_fusion
  162.1 0.6 reshape.466
  162.8 5.8 %all-to-all-done.4 = bf16[16,1,128]{2,1,0:T(2,128)(2,1)S(1)} async-done(((bf16[16,1,128]{2,1,0:T(2,128)(2,1)}), bf16[16,1,128]{2,1,0:T(2,128)(2,1)S(1)}, u32[]{:S(2)}, u32[]{:S(2)}) %all-to-all-start.4) | async-done | bytes 4128 | tf_op jit(solution)/shard_map/all_to_all | solution.py:144
  168.6 3.5 %all-to-all-start.2 = ((bf16[16,12,128]{2,1,0:T(8,128)(2,1)}), bf16[16,12,128]{2,1,0:T(8,128)(2,1)S(1)}, u32[]{:S(2)}, u32[]{:S(2)}) async-start(bf16[16,12,128]{2,1,0:T(8,128)(2,1)} %reshape.466), calls=%async_computation.2 | async-start | bytes 131072 | tf_op jit(solution)/shard_map/all_to_all | solution.py:143
  172.1 0.6 multiply_reduce_fusion.1
  173.5 0.2 fusion.64
  173.7 1.5 fusion.65
  175.2 1.5 fusion.66
  176.7 2.9 %all-to-all-done.2 = bf16[16,12,128]{2,1,0:T(8,128)(2,1)S(1)} async-done(((bf16[16,12,128]{2,1,0:T(8,128)(2,1)}), bf16[16,12,128]{2,1,0:T(8,128)(2,1)S(1)}, u32[]{:S(2)}, u32[]{:S(2)}) %all-to-all-start.2) | async-done | bytes 49184 | tf_op jit(solution)/shard_map/all_to_all | solution.py:143
  179.6 0.1 fusion.15
  179.9 1.5 fusion.9
  181.4 2.0 fusion.2
  183.3 3.8 %all-reduce.2 = (bf16[1,12,2048]{2,1,0:T(8,128)(2,1)S(1)}, bf16[1,1,2048]{2,1,0:T(2,128)(2,1)S(1)}) all-reduce(bf16[1,12,2048]{2,1,0:T(8,128)(2,1)S(1)} %fusion.2, bf16[1,1,2048]{2,1,0:T(2,128)(2,1)S(1)} %convert_element_type.218), channel_id=1, replica_groups=mesh['ep'=16,'tp'=2] {'tp'}, use_global_device_ids=true, to_apply=%region_8.9 | all-reduce | flops 26624 | bytes 106496 | tf_op jit(solution)/shard_map/psum | solution.py:157
  187.1 0.6 constant_dynamic-update-slice_fusion.15
  187.7 0.5 constant_dynamic-update-slice_fusion.14
  188.2 0.5 constant_dynamic-update-slice_fusion.13
  188.7 0.5 constant_dynamic-update-slice_fusion.12
  189.3 0.5 constant_dynamic-update-slice_fusion.11
  189.8 0.6 constant_dynamic-update-slice_fusion.10
  190.3 0.6 constant_dynamic-update-slice_fusion.9
  190.9 0.5 constant_dynamic-update-slice_fusion.8
  191.5 0.5 constant_dynamic-update-slice_fusion.7
  192.0 0.6 constant_dynamic-update-slice_fusion.6
  192.5 0.6 constant_dynamic-update-slice_fusion.5
  193.1 0.5 constant_dynamic-update-slice_fusion.4
  193.7 0.6 constant_dynamic-update-slice_fusion.3
  194.3 0.5 constant_dynamic-update-slice_fusion.2
  194.8 0.5 constant_dynamic-update-slice_fusion.1
  195.3 0.8 copy.102
  196.1 0.5 broadcast.256
  196.6 11.5 %reduce.9 = bf16[2048,12]{1,0:T(8,128)(2,1)S(1)} reduce(bf16[2048,1,12]{2,1,0:T(2,128)(2,1)S(1)} %bitcast.200, bf16[]{:T(256)} %broadcast.256), dimensions={1}, to_apply=%bitcast.183.reduce_sub_computation | reduce | bytes 98306
  208.2 1.6 reshape.513
  209.7 4.0 %all-to-all-start.3 = ((bf16[16,2,768]{2,1,0:T(2,128)(2,1)}), bf16[16,2,768]{2,1,0:T(2,128)(2,1)S(1)}, u32[]{:S(2)}, u32[]{:S(2)}) async-start(bf16[16,2,768]{2,1,0:T(2,128)(2,1)} %reshape.513), calls=%async_computation.3 | async-start | bytes 98304 | tf_op jit(solution)/shard_map/all_to_all | solution.py:163
  213.7 0.6 constant_dynamic-update-slice_fusion
  214.3 6.9 %all-to-all-done.3 = bf16[16,2,768]{2,1,0:T(2,128)(2,1)S(1)} async-done(((bf16[16,2,768]{2,1,0:T(2,128)(2,1)}), bf16[16,2,768]{2,1,0:T(2,128)(2,1)S(1)}, u32[]{:S(2)}, u32[]{:S(2)}) %all-to-all-start.3) | async-done | bytes 49184 | tf_op jit(solution)/shard_map/all_to_all | solution.py:163
  221.2 3.5 %all-to-all-start.5 = ((bf16[16,1,1,128]{3,2,1,0:T(2,128)(2,1)}), bf16[16,1,1,128]{3,2,1,0:T(2,128)(2,1)S(1)}, u32[]{:S(2)}, u32[]{:S(2)}) async-start(bf16[16,1,1,128]{3,2,1,0:T(2,128)(2,1)} %constant_dynamic-update-slice_fusion), calls=%async_computation.5 | async-start | bytes 16384 | tf_op jit(solution)/shard_map/all_to_all | solution.py:165
  224.7 1.4 reshape.514
  226.1 0.6 copy.103
  226.8 0.7 gather_fusion.1
  227.6 4.4 %all-to-all-done.5 = bf16[16,1,1,128]{3,2,1,0:T(2,128)(2,1)S(1)} async-done(((bf16[16,1,1,128]{3,2,1,0:T(2,128)(2,1)}), bf16[16,1,1,128]{3,2,1,0:T(2,128)(2,1)S(1)}, u32[]{:S(2)}, u32[]{:S(2)}) %all-to-all-start.5) | async-done | bytes 4128 | tf_op jit(solution)/shard_map/all_to_all | solution.py:165
  232.0 0.6 fusion.30
  (68 shorter events, 1.2 us)
Async XLA Ops:
  0.6 180.7 %copy-start = (bf16[1,256,2048]{2,1,0:T(8,128)(2,1)S(1)}, bf16[1,256,2048]{2,1,0:T(8,128)(2,1)}, u32[]{:S(2)}) copy-start(bf16[1,256,2048]{2,1,0:T(8,128)(2,1)} %param.38) | copy-start | bytes 3145732
  0.6 25.0 %copy-start.11 = (u32[32]{0:T(128)S(1)}, u32[32]{0:T(128)}, u32[]{:S(2)}) copy-start(u32[32]{0:T(128)} %constant.104) | copy-start | bytes 388
  0.7 24.9 %copy-start.9 = (f32[16,6]{0,1:T(8,128)S(1)}, f32[16,6]{0,1:T(8,128)}, u32[]{:S(2)}) copy-start(f32[16,6]{0,1:T(8,128)} %param.35) | copy-start | bytes 1156
  0.7 32.5 %copy-start.4 = (bf16[128,512]{1,0:T(8,128)(2,1)S(1)}, bf16[128,512]{1,0:T(8,128)(2,1)}, u32[]{:S(2)}) copy-start(bf16[128,512]{1,0:T(8,128)(2,1)} %param.26) | copy-start | bytes 393220
  0.7 32.6 %copy-start.5 = (bf16[128,512]{1,0:T(8,128)(2,1)S(1)}, bf16[128,512]{1,0:T(8,128)(2,1)}, u32[]{:S(2)}) copy-start(bf16[128,512]{1,0:T(8,128)(2,1)} %param.25) | copy-start | bytes 393220
  0.7 32.7 %copy-start.6 = (bf16[128,256]{1,0:T(8,128)(2,1)S(1)}, bf16[128,256]{1,0:T(8,128)(2,1)}, u32[]{:S(2)}) copy-start(bf16[128,256]{1,0:T(8,128)(2,1)} %param.24) | copy-start | bytes 196612
  0.7 32.8 %copy-start.7 = (bf16[128,256]{1,0:T(8,128)(2,1)S(1)}, bf16[128,256]{1,0:T(8,128)(2,1)}, u32[]{:S(2)}) copy-start(bf16[128,256]{1,0:T(8,128)(2,1)} %param.23) | copy-start | bytes 196612
  0.7 111.7 %copy-start.3 = (f32[1,1,256,512]{3,2,1,0:T(8,128)S(1)}, f32[1,1,256,512]{3,2,1,0:T(8,128)}, u32[]{:S(2)}) copy-start(f32[1,1,256,512]{3,2,1,0:T(8,128)} %param.30) | copy-start | bytes 1572868
  4.2 22.0 %all-to-all-start.1 = ((bf16[1,16,128]{2,0,1:T(2,128)(2,1)}), bf16[1,16,128]{2,0,1:T(2,128)(2,1)S(1)}, u32[]{:S(2)}, u32[]{:S(2)}) async-start(bf16[1,16,128]{2,0,1:T(2,128)(2,1)} %convert_bitcast_fusion.3), calls=%async_computation.1 | async-start | bytes 16384 | tf_op jit(solution)/shard_map/all_to_all | solution.py:76
  13.6 100.7 %copy-start.10 = (f32[512]{0:T(512)S(1)}, f32[512]{0:T(512)}, u32[]{:S(2)}) copy-start(f32[512]{0:T(512)} %param.31) | copy-start | bytes 6148
  25.5 147.9 %copy-start.8 = (f32[2048]{0:T(1024)S(1)}, f32[2048]{0:T(1024)}, u32[]{:S(2)}) copy-start(f32[2048]{0:T(1024)} %param.33) | copy-start | bytes 24580
  25.5 148.0 %copy-start.2 = (bf16[2048,256]{1,0:T(8,128)(2,1)S(1)}, bf16[2048,256]{1,0:T(8,128)(2,1)}, u32[]{:S(2)}) copy-start(bf16[2048,256]{1,0:T(8,128)(2,1)} %param.39) | copy-start | bytes 3145732
  26.2 131.1 %all-to-all-start = ((bf16[1,16,128]{2,0,1:T(2,128)(2,1)}), bf16[1,16,128]{2,0,1:T(2,128)(2,1)S(1)}, u32[]{:S(2)}, u32[]{:S(2)}) async-start(bf16[1,16,128]{2,0,1:T(2,128)(2,1)} %bitcast), calls=%async_computation | async-start | bytes 16384 | tf_op jit(solution)/shard_map/all_to_all | solution.py:75
  112.6 64.1 %copy-start.1 = (f32[1,1,256,512]{3,2,1,0:T(8,128)}, f32[1,1,256,512]{3,2,1,0:T(8,128)S(1)}, u32[]{:S(2)}) copy-start(f32[1,1,256,512]{3,2,1,0:T(8,128)S(1)} %multiply_add_fusion) | copy-start | bytes 1572868
  157.9 10.7 %all-to-all-start.4 = ((bf16[16,1,128]{2,1,0:T(2,128)(2,1)}), bf16[16,1,128]{2,1,0:T(2,128)(2,1)S(1)}, u32[]{:S(2)}, u32[]{:S(2)}) async-start(bf16[16,1,128]{2,1,0:T(2,128)(2,1)} %copy.106), calls=%async_computation.4 | async-start | bytes 16384 | tf_op jit(solution)/shard_map/all_to_all | solution.py:144
  168.6 11.0 %all-to-all-start.2 = ((bf16[16,12,128]{2,1,0:T(8,128)(2,1)}), bf16[16,12,128]{2,1,0:T(8,128)(2,1)S(1)}, u32[]{:S(2)}, u32[]{:S(2)}) async-start(bf16[16,12,128]{2,1,0:T(8,128)(2,1)} %reshape.466), calls=%async_computation.2 | async-start | bytes 131072 | tf_op jit(solution)/shard_map/all_to_all | solution.py:143
  209.7 11.5 %all-to-all-start.3 = ((bf16[16,2,768]{2,1,0:T(2,128)(2,1)}), bf16[16,2,768]{2,1,0:T(2,128)(2,1)S(1)}, u32[]{:S(2)}, u32[]{:S(2)}) async-start(bf16[16,2,768]{2,1,0:T(2,128)(2,1)} %reshape.513), calls=%async_computation.3 | async-start | bytes 98304 | tf_op jit(solution)/shard_map/all_to_all | solution.py:163
  221.2 10.7 %all-to-all-start.5 = ((bf16[16,1,1,128]{3,2,1,0:T(2,128)(2,1)}), bf16[16,1,1,128]{3,2,1,0:T(2,128)(2,1)S(1)}, u32[]{:S(2)}, u32[]{:S(2)}) async-start(bf16[16,1,1,128]{3,2,1,0:T(2,128)(2,1)} %constant_dynamic-update-slice_fusion), calls=%async_computation.5 | async-start | bytes 16384 | tf_op jit(solution)/shard_map/all_to_all | solution.py:165
